TPU v7x, 32 devices: a whole 2x2x4 slice. The times are simulated.
32 devices in a mesh: fs: 4 (over y, x), tp: 8 (over z, core).
Axes of the slice: x: 2, y: 2, z: 4, core: 2. Of those that a mesh axis runs over, the one named last changes fastest.
Arguments:
- tokens: bfloat16 [4096, 2048], P(('fs', 'tp')), may hold values from -6 to 6
- gate_weight: bfloat16 [2048, 5632], P('fs', 'tp'), may hold values from -0.125 to 0.125
- up_weight: bfloat16 [2048, 5632], P('fs', 'tp'), may hold values from -0.125 to 0.125
- down_weight: bfloat16 [5632, 2048], P('tp', 'fs'), may hold values from -0.078125 to 0.078125
- grad_out: bfloat16 [4096, 2048], P(('fs', 'tp')), may hold values from -6 to 6
Outputs:
- grad_input: bfloat16 [4096, 2048], P(('fs', 'tp'))
- grad_gate: float32 [2048, 5632], P('fs', 'tp')
- grad_up: float32 [2048, 5632], P('fs', 'tp')
- grad_down: float32 [5632, 2048], P('tp', 'fs')
All inputs are finite; a program needn't handle non-finite values.
Results may differ from a plain program's by a relative error of at most 0.0049.
Values may be sent and summed in bfloat16 or wider, within the bound.
A program may use at most 128 MiB of HBM per device.

v0:
```python
import jax
import jax.numpy as jnp
from jax import lax
from jax.sharding import PartitionSpec as P


def over_rows(left, right):
    return lax.dot_general(
        left, right, (((0,), (0,)), ((), ())), preferred_element_type=jnp.float32
    )


def over_cols(left, right):
    return lax.dot_general(
        left, right, (((1,), (1,)), ((), ())), preferred_element_type=jnp.float32
    )


def body(tokens, gate_weight, up_weight, down_weight, grad_out):
    tok_all, cot_all = (
        lax.all_gather(tokens, "tp", axis=0, tiled=True),
        lax.all_gather(grad_out, "tp", axis=0, tiled=True),
    )
    gate_full, up_full = (
        lax.all_gather(gate_weight, "fs", axis=0, tiled=True),
        lax.all_gather(up_weight, "fs", axis=0, tiled=True),
    )
    down_full = lax.all_gather(down_weight, "fs", axis=1, tiled=True)
    gate_pre = jnp.dot(tok_all, gate_full, preferred_element_type=jnp.float32)
    up_pre = jnp.dot(tok_all, up_full, preferred_element_type=jnp.float32)
    sig_gate = jax.nn.sigmoid(gate_pre)
    active = gate_pre * sig_gate
    hidden = (active * up_pre).astype(jnp.bfloat16)
    d_hidden = over_cols(cot_all, down_full)
    d_gate = (d_hidden * up_pre * sig_gate * (1.0 + gate_pre * (1.0 - sig_gate))).astype(
        jnp.bfloat16
    )
    d_up = (d_hidden * active).astype(jnp.bfloat16)
    grad_input = lax.psum_scatter(
        over_cols(d_gate, gate_full) + over_cols(d_up, up_full),
        "tp",
        scatter_dimension=0,
        tiled=True,
    ).astype(jnp.bfloat16)
    width = gate_full.shape[1]
    summed = lax.psum_scatter(
        jnp.concatenate(
            [over_rows(tok_all, d_gate), over_rows(tok_all, d_up), over_rows(cot_all, hidden)],
            axis=1,
        ),
        "fs",
        scatter_dimension=0,
        tiled=True,
    )
    grad_gate = summed[:, :width]
    grad_up = summed[:, width : 2 * width]
    grad_down = summed[:, 2 * width :].T
    return (grad_input, grad_gate, grad_up, grad_down)


def solution(mesh):
    in_specs = (
        P(("fs", "tp"), None),
        P("fs", "tp"),
        P("fs", "tp"),
        P("tp", "fs"),
        P(("fs", "tp"), None),
    )
    out_specs = (P(("fs", "tp"), None), P("fs", "tp"), P("fs", "tp"), P("tp", "fs"))
    return jax.shard_map(body, mesh=mesh, in_specs=in_specs, out_specs=out_specs, check_vma=False)
```

profile of v0, /device:TPU:0, one launch (start us, length us, event | category | flops | bytes accessed | tf_op | source)
XLA Modules:
  0.0 514.1 jit_solution(16898894607041836768)
XLA Ops:
  7.2 0.7 all-gather.12.cloned.1.call-update
  7.9 0.7 all-gather.10.cloned.1.call-update
  8.7 0.7 all-gather.14.cloned.1.call-update
  10.0 0.5 all-gather.6.cloned.1.call-update
  10.6 43.5 %all-gather.12.cloned.1.call-done = bf16[2048,704]{0,1:T(8,128)(2,1)} async-done(((bf16[512,704]{0,1:T(8,128)(2,1)}), bf16[2048,704]{0,1:T(8,128)(2,1)}) %all-gather.12.cloned.1.call-update) | async-done | bytes 2883600 | tf_op jit(solution)/shard_map/all_gather | solution.py:26
  54.1 48.5 %all-gather.10.cloned.1.call-done = bf16[1024,2048]{1,0:T(8,128)(2,1)} async-done(((bf16[128,2048]{1,0:T(8,128)(2,1)}), bf16[1024,2048]{1,0:T(8,128)(2,1)}) %all-gather.10.cloned.1.call-update) | async-done | bytes 4194320 | tf_op jit(solution)/shard_map/all_gather | solution.py:21
  102.6 7.8 %fusion.3 = f32[1024,704]{0,1:T(8,128)} fusion(bf16[1024,2048]{1,0:T(8,128)(2,1)} %all-gather.10.cloned.1.call-done, bf16[2048,704]{0,1:T(8,128)(2,1)} %all-gather.12.cloned.1.call-done), kind=kOutput, calls=%fused_computation.12 | convolution fusion | flops 2952790016 | bytes 9961472 | tf_op jit(solution)/shard_map/dot_general | solution.py:30
  110.4 34.4 %all-gather.14.cloned.1.call-done = bf16[2048,704]{0,1:T(8,128)(2,1)} async-done(((bf16[512,704]{0,1:T(8,128)(2,1)}), bf16[2048,704]{0,1:T(8,128)(2,1)}) %all-gather.14.cloned.1.call-update) | async-done | bytes 2883600 | tf_op jit(solution)/shard_map/all_gather | solution.py:25
  144.8 7.9 %fusion.4 = f32[1024,704]{0,1:T(8,128)} fusion(bf16[1024,2048]{1,0:T(8,128)(2,1)} %all-gather.10.cloned.1.call-done, bf16[2048,704]{0,1:T(8,128)(2,1)} %all-gather.14.cloned.1.call-done), kind=kOutput, calls=%fused_computation.13 | convolution fusion | flops 2952790016 | bytes 9961472 | tf_op jit(solution)/shard_map/dot_general | solution.py:29
  152.7 35.3 %all-gather.8.cloned.1.call-done = bf16[704,2048]{1,0:T(8,128)(2,1)} async-done(((bf16[704,512]{1,0:T(8,128)(2,1)}), bf16[704,2048]{1,0:T(8,128)(2,1)}) %all-gather.8.cloned.1.call-update) | async-done | bytes 2883600 | tf_op jit(solution)/shard_map/all_gather | solution.py:28
  188.1 48.3 %all-gather.6.cloned.1.call-done = bf16[1024,2048]{1,0:T(8,128)(2,1)} async-done(((bf16[128,2048]{1,0:T(8,128)(2,1)}), bf16[1024,2048]{1,0:T(8,128)(2,1)}) %all-gather.6.cloned.1.call-update) | async-done | bytes 4194320 | tf_op jit(solution)/shard_map/all_gather | solution.py:22
  236.4 8.6 %multiply_convert_fusion.1 = (bf16[1024,704]{0,1:T(8,128)(2,1)S(1)}, bf16[1024,704]{0,1:T(8,128)(2,1)S(1)}) fusion(f32[1024,704]{0,1:T(8,128)} %fusion.4, f32[1024,704]{0,1:T(8,128)} %fusion.3, bf16[1024,2048]{1,0:T(8,128)(2,1)} %all-gather.6.cloned.1.call-done, bf16[704,2048]{1,0:T(8,128)(2,1)} %all-gather.8.cloned.1.call-done), kind=kOutput, calls=%fused_computation.6 | convolution fusion | flops 2962161664 | bytes 15728640 | tf_op jit(solution)/shard_map/dot_general | solution.py:14
  245.1 3.5 fusion.5
  248.6 6.1 %convolution_add_fusion = f32[1024,2048]{1,0:T(8,128)} fusion(f32[1024,2048]{1,0:T(8,128)S(1)} %fusion.5, bf16[1024,704]{0,1:T(8,128)(2,1)S(1)} %get-tuple-element.4, bf16[2048,704]{0,1:T(8,128)(2,1)S(1)} %copy-done.2), kind=kOutput, calls=%fused_computation.1 | convolution fusion | flops 2954887168 | bytes 21102592 | tf_op jit(solution)/shard_map/dot_general | solution.py:14
  254.8 1.3 copy-done.5
  256.1 5.1 convolution_bitcast_fusion.1
  261.2 3.2 convolution_bitcast_fusion.2
  264.4 0.7 copy-done.9
  265.1 3.2 convolution_bitcast_fusion
  268.3 6.5 %pad_maximum_fusion = f32[2048,2112]{0,1:T(8,128)} fusion(f32[2048,704]{0,1:T(8,128)S(1)} %convolution_bitcast_fusion, f32[2048,704]{0,1:T(8,128)S(1)} %convolution_bitcast_fusion.1, f32[2048,704]{0,1:T(8,128)S(1)} %convolution_bitcast_fusion.2), kind=kLoop, calls=%fused_computation | loop fusion | flops 8650752 | bytes 34603008 | tf_op jit(solution)/shard_map/concatenate | solution.py:47
  274.9 68.4 %reduce-scatter.3.cloned.1.call-done = f32[128,2048]{1,0:T(8,128)} async-done(((f32[1024,2048]{1,0:T(8,128)}), f32[128,2048]{1,0:T(8,128)}) %reduce-scatter.3.cloned.1.call-update) | async-done | bytes 1048592 | tf_op jit(solution)/shard_map/reduce_scatter | solution.py:39
  343.2 2.1 convert_element_type.14
  345.3 157.5 %reduce-scatter.5.cloned.1.call-done = f32[512,2112]{0,1:T(8,128)} async-done(((f32[2048,2112]{0,1:T(8,128)}), f32[512,2112]{0,1:T(8,128)}) %reduce-scatter.5.cloned.1.call-update) | async-done | bytes 4325392 | tf_op jit(solution)/shard_map/reduce_scatter | solution.py:46
  502.8 4.4 slice_bitcast_fusion
  (28 shorter events, 0.9 us)
Async XLA Ops:
  7.2 46.9 %all-gather.12.cloned.1.call-start = ((), (), s32[]{:S(2)}) async-start(), calls=%async_computation.5 | async-start | bytes 3604480 | tf_op jit(solution)/shard_map/all_gather | solution.py:26
  7.9 94.7 %all-gather.10.cloned.1.call-start = ((), (), s32[]{:S(2)}) async-start(), calls=%async_computation.4 | async-start | bytes 4718592 | tf_op jit(solution)/shard_map/all_gather | solution.py:21
  8.6 136.2 %all-gather.14.cloned.1.call-start = ((), (), s32[]{:S(2)}) async-start(), calls=%async_computation.6 | async-start | bytes 3604480 | tf_op jit(solution)/shard_map/all_gather | solution.py:25
  9.4 178.7 %all-gather.8.cloned.1.call-start = ((), (), s32[]{:S(2)}) async-start(), calls=%async_computation.3 | async-start | bytes 3604480 | tf_op jit(solution)/shard_map/all_gather | solution.py:28
  10.0 226.4 %all-gather.6.cloned.1.call-start = ((), (), s32[]{:S(2)}) async-start(), calls=%async_computation.2 | async-start | bytes 4718592 | tf_op jit(solution)/shard_map/all_gather | solution.py:22
  10.5 332.7 %reduce-scatter.3.cloned.1.call-start = ((), (), s32[]{:S(2)}) async-start(), calls=%async_computation.7 | async-start | bytes 9437184 | tf_op jit(solution)/shard_map/reduce_scatter | solution.py:39
  152.7 92.3 %copy-start.3 = (bf16[2048,704]{0,1:T(8,128)(2,1)S(1)}, bf16[2048,704]{0,1:T(8,128)(2,1)}, u32[]{:S(2)}) copy-start(bf16[2048,704]{0,1:T(8,128)(2,1)} %all-gather.14.cloned.1.call-done) | copy-start | bytes 8650756
  245.0 3.6 copy-start.6
  245.0 3.6 copy-start.4
  245.1 3.6 copy-start.2
  254.7 1.4 copy-start.5
  254.7 6.4 %copy-start.7 = (bf16[1024,704]{0,1:T(8,128)(2,1)S(1)}, bf16[1024,704]{0,1:T(8,128)(2,1)}, u32[]{:S(2)}) copy-start(bf16[1024,704]{0,1:T(8,128)(2,1)} %copy-done.6) | copy-start | bytes 4325380
  254.8 248.1 %reduce-scatter.5.cloned.1.call-start = ((), (), s32[]{:S(2)}) async-start(), calls=%async_computation.8 | async-start | bytes 21626880 | tf_op jit(solution)/shard_map/reduce_scatter | solution.py:46
  256.1 5.1 copy-start
  261.2 3.2 copy-start.1
  261.2 3.2 copy-start.8
  261.2 3.9 copy-start.9
Sparse Core Ops, SparseCore 0:
  9.8 44.2 all-gather.11
  55.7 46.8 all-gather.9
  104.4 40.3 all-gather.13
  146.5 41.5 all-gather.7
  189.5 46.8 all-gather.5
  254.9 88.3 reduce-scatter.2
  346.4 156.4 reduce-scatter.4
where the time goes:
time: 514 us
  waiting for transfers between devices  439 us (85%)
  matrix products  45.4 us (9%)
  between operations  14.3 us (3%)
  other arithmetic  8.6 us (2%)
  local copies, waits for them, and re-layouts  6.37 us (1%)
    reduce_scatter x1, waiting for transfers between devices, body(): lax.psum_scatter(jnp.concatenate([over_rows(tok_all, d_gate), over_rows(t...  158 us
    reduce_scatter x1, waiting for transfers between devices, body(): lax.psum_scatter(over_cols(d_gate, gate_full) + over_cols(d_up, up_full),...  68.4 us
    all_gather x1, waiting for transfers between devices, body(): lax.all_gather(tokens, 'tp', axis=0, tiled=True)  48.5 us
    all_gather x1, waiting for transfers between devices, body(): lax.all_gather(grad_out, 'tp', axis=0, tiled=True)  48.3 us
    all_gather x1, waiting for transfers between devices, body(): lax.all_gather(up_weight, 'fs', axis=0, tiled=True)  43.5 us
    all_gather x1, waiting for transfers between devices, body(): down_full = lax.all_gather(down_weight, 'fs', axis=1, tiled=True)  35.3 us
    all_gather x1, waiting for transfers between devices, body(): lax.all_gather(gate_weight, 'fs', axis=0, tiled=True)  34.4 us
    dot_general x3, matrix products, over_cols(): lax.dot_general(left, right, (((1,), (1,)), ((), ())), preferred_element_...  18.2 us
  transfers between devices with their start and end apart: 7, of which 7 were waited for; matrix products, arithmetic and copies ran while one was open for 7% of the time, Pallas kernels for 0%

commit v1 on v0

--- a/solution.py
+++ b/solution.py
@@ -18,7 +18,9 @@
 
 def body(tokens, gate_weight, up_weight, down_weight, grad_out):
     tok_all, cot_all = (
-        lax.all_gather(tokens, "tp", axis=0, tiled=True),
+        jnp.concatenate(
+            lax.all_to_all(jnp.stack([tokens] * lax.axis_size("tp")), "tp", 0, 0), axis=0
+        ),
         lax.all_gather(grad_out, "tp", axis=0, tiled=True),
     )
     gate_full, up_full = (

time: 514 us -> 467 us (0.909)
  waiting for transfers between devices: 439 us -> 381 us
  starting transfers between devices: 0.27 us -> 6.58 us
    all_to_all x0 -> x1, waiting for transfers between devices: none -> 59.3 us  [body(): lax.all_to_all(jnp.stack([tokens] * lax.axis_size('tp')), 'tp', 0, 0)]
    all_gather x1 -> x0, waiting for transfers between devices: 48.5 us -> none  [body(): lax.all_gather(tokens, 'tp', axis=0, tiled=True)]
    all_gather x1, waiting for transfers between devices: 43.5 us -> 0.01 us  [body(): lax.all_gather(up_weight, 'fs', axis=0, tiled=True)]
    all_gather x1, waiting for transfers between devices: 35.3 us -> 11.7 us  [body(): down_full = lax.all_gather(down_weight, 'fs', axis=1, tiled=True)]
    all_to_all x0 -> x1, starting transfers between devices: none -> 6.35 us  [body(): lax.all_to_all(jnp.stack([tokens] * lax.axis_size('tp')), 'tp', 0, 0)]
  transfers between devices with their start and end apart: 7 -> 7, of which waited for: 7 -> 6; matrix products, arithmetic and copies ran while one was open for 7% -> 9% of each run, Pallas kernels for 0% -> 0%
where the time goes in v1:
time: 467 us
  waiting for transfers between devices  381 us (82%)
  matrix products  47.4 us (10%)
  between operations  14.3 us (3%)
  local copies, waits for them, and re-layouts  9.28 us (2%)
  other arithmetic  8.62 us (2%)
  starting transfers between devices  6.58 us (1%)
    reduce_scatter x1, waiting for transfers between devices, body(): lax.psum_scatter(jnp.concatenate([over_rows(tok_all, d_gate), over_rows(t...  157 us
    reduce_scatter x1, waiting for transfers between devices, body(): lax.psum_scatter(over_cols(d_gate, gate_full) + over_cols(d_up, up_full),...  67.2 us
    all_to_all x1, waiting for transfers between devices, body(): lax.all_to_all(jnp.stack([tokens] * lax.axis_size('tp')), 'tp', 0, 0)  59.3 us
    all_gather x1, waiting for transfers between devices, body(): lax.all_gather(grad_out, 'tp', axis=0, tiled=True)  48.4 us
    all_gather x1, waiting for transfers between devices, body(): lax.all_gather(gate_weight, 'fs', axis=0, tiled=True)  34.2 us
    dot_general x3, matrix products, over_cols(): lax.dot_general(left, right, (((1,), (1,)), ((), ())), preferred_element_...  18.3 us
    dot_general x3, matrix products, over_rows(): lax.dot_general(left, right, (((0,), (0,)), ((), ())), preferred_element_...  13.2 us
    all_gather x1, waiting for transfers between devices, body(): down_full = lax.all_gather(down_weight, 'fs', axis=1, tiled=True)  11.7 us
  transfers between devices with their start and end apart: 7, of which 6 were waited for; matrix products, arithmetic and copies ran while one was open for 9% of the time, Pallas kernels for 0%

profile of v1, /device:TPU:0, one launch (start us, length us, event | category | flops | bytes accessed | tf_op | source)
XLA Modules:
  0.0 466.8 jit_solution(4492660788380723478)
XLA Ops:
  7.2 0.7 all-gather.11.cloned.1.call-update
  7.9 0.7 all-gather.9.cloned.1.call-update
  8.7 0.7 all-gather.7.cloned.1.call-update
  9.4 3.6 stack.2
  12.9 6.4 %all-to-all-start = ((bf16[8,128,2048]{2,1,0:T(8,128)(2,1)}), bf16[8,128,2048]{2,1,0:T(8,128)(2,1)}, u32[]{:S(2)}, u32[]{:S(2)}) async-start(bf16[8,128,2048]{2,1,0:T(8,128)(2,1)} %stack.2), calls=%async_computation | async-start | bytes 8388608 | tf_op jit(solution)/shard_map/all_to_all | solution.py:22
  19.3 0.5 all-gather.5.cloned.1.call-update
  19.9 34.2 %all-gather.11.cloned.1.call-done = bf16[2048,704]{0,1:T(8,128)(2,1)} async-done(((bf16[512,704]{0,1:T(8,128)(2,1)}), bf16[2048,704]{0,1:T(8,128)(2,1)}) %all-gather.11.cloned.1.call-update) | async-done | bytes 2883600 | tf_op jit(solution)/shard_map/all_gather | solution.py:27
  54.1 59.3 %all-to-all-done = bf16[8,128,2048]{2,1,0:T(8,128)(2,1)} async-done(((bf16[8,128,2048]{2,1,0:T(8,128)(2,1)}), bf16[8,128,2048]{2,1,0:T(8,128)(2,1)}, u32[]{:S(2)}, u32[]{:S(2)}) %all-to-all-start) | async-done | bytes 4194336 | tf_op jit(solution)/shard_map/all_to_all | solution.py:22
  113.4 7.9 %fusion.4 = f32[1024,704]{0,1:T(8,128)} fusion(bf16[1024,2048]{1,0:T(8,128)(2,1)} %bitcast, bf16[2048,704]{0,1:T(8,128)(2,1)} %all-gather.11.cloned.1.call-done), kind=kOutput, calls=%fused_computation.13 | convolution fusion | flops 2952790016 | bytes 9961472 | tf_op jit(solution)/shard_map/dot_general | solution.py:31
  121.3 8.0 %fusion.3 = f32[1024,704]{0,1:T(8,128)} fusion(bf16[1024,2048]{1,0:T(8,128)(2,1)} %bitcast, bf16[2048,704]{0,1:T(8,128)(2,1)} %all-gather.9.cloned.1.call-done), kind=kOutput, calls=%fused_computation.12 | convolution fusion | flops 2952790016 | bytes 9961472 | tf_op jit(solution)/shard_map/dot_general | solution.py:32
  129.2 11.7 %all-gather.7.cloned.1.call-done = bf16[704,2048]{1,0:T(8,128)(2,1)} async-done(((bf16[704,512]{1,0:T(8,128)(2,1)}), bf16[704,2048]{1,0:T(8,128)(2,1)}) %all-gather.7.cloned.1.call-update) | async-done | bytes 2883600 | tf_op jit(solution)/shard_map/all_gather | solution.py:30
  140.9 48.4 %all-gather.5.cloned.1.call-done = bf16[1024,2048]{1,0:T(8,128)(2,1)} async-done(((bf16[128,2048]{1,0:T(8,128)(2,1)}), bf16[1024,2048]{1,0:T(8,128)(2,1)}) %all-gather.5.cloned.1.call-update) | async-done | bytes 4194320 | tf_op jit(solution)/shard_map/all_gather | solution.py:24
  189.2 8.7 %multiply_convert_fusion.1 = (bf16[1024,704]{0,1:T(8,128)(2,1)S(1)}, bf16[1024,704]{0,1:T(8,128)(2,1)S(1)}) fusion(f32[1024,704]{0,1:T(8,128)} %fusion.4, f32[1024,704]{0,1:T(8,128)} %fusion.3, bf16[1024,2048]{1,0:T(8,128)(2,1)} %all-gather.5.cloned.1.call-done, bf16[704,2048]{1,0:T(8,128)(2,1)} %all-gather.7.cloned.1.call-done), kind=kOutput, calls=%fused_computation.6 | convolution fusion | flops 2962161664 | bytes 15728640 | tf_op jit(solution)/shard_map/dot_general | solution.py:14
  198.0 3.5 fusion.5
  201.6 6.0 %convolution_add_fusion = f32[1024,2048]{1,0:T(8,128)} fusion(f32[1024,2048]{1,0:T(8,128)S(1)} %fusion.5, bf16[1024,704]{0,1:T(8,128)(2,1)S(1)} %get-tuple-element.4, bf16[2048,704]{0,1:T(8,128)(2,1)S(1)} %copy-done.2), kind=kOutput, calls=%fused_computation.1 | convolution fusion | flops 2954887168 | bytes 21102592 | tf_op jit(solution)/shard_map/dot_general | solution.py:14
  207.7 1.3 copy-done.4
  209.0 4.9 %convolution_bitcast_fusion.1 = f32[2048,704]{0,1:T(8,128)S(1)} fusion(bf16[1024,704]{0,1:T(8,128)(2,1)S(1)} %copy-done.4, bf16[1024,2048]{1,0:T(8,128)(2,1)} %bitcast), kind=kOutput, calls=%fused_computation.3 | convolution fusion | flops 2952790016 | bytes 11403264 | tf_op jit(solution)/shard_map/dot_general | solution.py:8
  214.0 5.1 %convolution_bitcast_fusion.2 = f32[2048,704]{0,1:T(8,128)S(1)} fusion(bf16[1024,704]{0,1:T(8,128)(2,1)S(1)} %copy-done.6, bf16[1024,2048]{1,0:T(8,128)(2,1)} %bitcast), kind=kOutput, calls=%fused_computation.4 | convolution fusion | flops 2952790016 | bytes 11403264 | tf_op jit(solution)/shard_map/dot_general | solution.py:8
  219.1 3.2 convolution_bitcast_fusion
  222.3 6.5 %pad_maximum_fusion = f32[2048,2112]{0,1:T(8,128)} fusion(f32[2048,704]{0,1:T(8,128)S(1)} %convolution_bitcast_fusion, f32[2048,704]{0,1:T(8,128)S(1)} %convolution_bitcast_fusion.1, f32[2048,704]{0,1:T(8,128)S(1)} %convolution_bitcast_fusion.2), kind=kLoop, calls=%fused_computation | loop fusion | flops 8650752 | bytes 34603008 | tf_op jit(solution)/shard_map/concatenate | solution.py:49
  228.9 67.2 %reduce-scatter.3.cloned.1.call-done = f32[128,2048]{1,0:T(8,128)} async-done(((f32[1024,2048]{1,0:T(8,128)}), f32[128,2048]{1,0:T(8,128)}) %reduce-scatter.3.cloned.1.call-update) | async-done | bytes 1048592 | tf_op jit(solution)/shard_map/reduce_scatter | solution.py:41
  296.2 2.1 convert_element_type.14
  298.2 157.4 %reduce-scatter.5.cloned.1.call-done = f32[512,2112]{0,1:T(8,128)} async-done(((f32[2048,2112]{0,1:T(8,128)}), f32[512,2112]{0,1:T(8,128)}) %reduce-scatter.5.cloned.1.call-update) | async-done | bytes 4325392 | tf_op jit(solution)/shard_map/reduce_scatter | solution.py:48
  455.6 4.4 slice_bitcast_fusion
  (26 shorter events, 0.3 us)
Async XLA Ops:
  7.2 46.9 %all-gather.11.cloned.1.call-start = ((), (), s32[]{:S(2)}) async-start(), calls=%async_computation.6 | async-start | bytes 3604480 | tf_op jit(solution)/shard_map/all_gather | solution.py:27
  7.9 113.4 %all-gather.9.cloned.1.call-start = ((), (), s32[]{:S(2)}) async-start(), calls=%async_computation.5 | async-start | bytes 3604480 | tf_op jit(solution)/shard_map/all_gather | solution.py:28
  8.6 132.2 %all-gather.7.cloned.1.call-start = ((), (), s32[]{:S(2)}) async-start(), calls=%async_computation.4 | async-start | bytes 3604480 | tf_op jit(solution)/shard_map/all_gather | solution.py:30
  12.9 100.4 %all-to-all-start = ((bf16[8,128,2048]{2,1,0:T(8,128)(2,1)}), bf16[8,128,2048]{2,1,0:T(8,128)(2,1)}, u32[]{:S(2)}, u32[]{:S(2)}) async-start(bf16[8,128,2048]{2,1,0:T(8,128)(2,1)} %stack.2), calls=%async_computation | async-start | bytes 8388608 | tf_op jit(solution)/shard_map/all_to_all | solution.py:22
  19.3 170.0 %all-gather.5.cloned.1.call-start = ((), (), s32[]{:S(2)}) async-start(), calls=%async_computation.3 | async-start | bytes 4718592 | tf_op jit(solution)/shard_map/all_gather | solution.py:24
  19.9 276.3 %reduce-scatter.3.cloned.1.call-start = ((), (), s32[]{:S(2)}) async-start(), calls=%async_computation.7 | async-start | bytes 9437184 | tf_op jit(solution)/shard_map/reduce_scatter | solution.py:41
  129.2 68.8 %copy-start.1 = (bf16[2048,704]{0,1:T(8,128)(2,1)S(1)}, bf16[2048,704]{0,1:T(8,128)(2,1)}, u32[]{:S(2)}) copy-start(bf16[2048,704]{0,1:T(8,128)(2,1)} %all-gather.11.cloned.1.call-done) | copy-start | bytes 8650756
  198.0 3.6 copy-start.5
  198.0 3.6 copy-start.3
  198.0 3.6 copy-start.2
  207.6 1.4 copy-start.4
  207.7 6.3 %copy-start.6 = (bf16[1024,704]{0,1:T(8,128)(2,1)S(1)}, bf16[1024,704]{0,1:T(8,128)(2,1)}, u32[]{:S(2)}) copy-start(bf16[1024,704]{0,1:T(8,128)(2,1)} %copy-done.5) | copy-start | bytes 4325380
  207.7 247.9 %reduce-scatter.5.cloned.1.call-start = ((), (), s32[]{:S(2)}) async-start(), calls=%async_computation.8 | async-start | bytes 21626880 | tf_op jit(solution)/shard_map/reduce_scatter | solution.py:48
  213.9 5.1 %copy-start = (bf16[1024,2048]{1,0:T(8,128)(2,1)S(1)}, bf16[1024,2048]{1,0:T(8,128)(2,1)}, u32[]{:S(2)}) copy-start(bf16[1024,2048]{1,0:T(8,128)(2,1)} %all-gather.5.cloned.1.call-done) | copy-start | bytes 12582916
  214.0 5.1 %copy-start.7 = (f32[1024,704]{0,1:T(8,128)S(1)}, f32[1024,704]{0,1:T(8,128)}, u32[]{:S(2)}) copy-start(f32[1024,704]{0,1:T(8,128)} %fusion.4) | copy-start | bytes 8650756
  214.0 5.2 %copy-start.8 = (f32[1024,704]{0,1:T(8,128)S(1)}, f32[1024,704]{0,1:T(8,128)}, u32[]{:S(2)}) copy-start(f32[1024,704]{0,1:T(8,128)} %fusion.3) | copy-start | bytes 8650756
Sparse Core Ops, SparseCore 0:
  9.8 44.2 all-gather.10
  55.9 41.5 all-gather.8
  99.3 41.5 all-gather.6
  142.4 46.8 all-gather.4
  207.8 88.3 reduce-scatter.2
  299.1 156.4 reduce-scatter.4
